TPU v7x, 256 devices: a whole 4x4x8 slice. The times are simulated.
256 devices in a mesh: fs: 16 (over y, x), tp: 16 (over z, core).
Axes of the slice: x: 4, y: 4, z: 8, core: 2. Of those that a mesh axis runs over, the one named last changes fastest.
Arguments:
- stream_in: bfloat16 [32768, 4096], P(('fs', 'tp')), may hold values from -6 to 6
- mixer_out: bfloat16 [32768, 4096], P(('fs', 'tp')), may hold values from -6 to 6
- mix_gain: float32 [4096], replicated, may hold values from 0.1 to 1.9
- pre_gain: float32 [4096], replicated, may hold values from 0.1 to 1.9
- gate_weight: float32 [4096, 6144], P('fs', 'tp'), may hold values from -0.09375 to 0.09375
- up_weight: float32 [4096, 6144], P('fs', 'tp'), may hold values from -0.09375 to 0.09375
- gate_scale: float32 [6144], P('tp'), may hold values from 0.5 to 2
- up_scale: float32 [6144], P('tp'), may hold values from 0.5 to 2
Outputs:
- hidden: bfloat16 [32768, 6144], P('fs', 'tp')
- stream: bfloat16 [32768, 4096], P(('fs', 'tp'))
All inputs are finite; a program needn't handle non-finite values.
Results may differ from a plain program's by a relative error of at most 0.0082.
Values may be sent and summed in bfloat16 or wider, within the bound.
A program may use at most 128 MiB of HBM per device.

v0:
```python
import jax
import jax.numpy as jnp
from jax import lax
from jax.sharding import PartitionSpec as P

epsilon = 1e-06


def in_one_piece(arrays, axis, dim, along):
    both = jnp.concatenate(arrays, axis=along)
    out, at, finished = (lax.all_gather(both, axis, axis=dim, tiled=True), 0, [])
    for a in arrays:
        finished.append(lax.slice_in_dim(out, at, at + a.shape[along], axis=along))
        at += a.shape[along]
    return tuple(finished)


def rms_scaled(values, gain):
    return values * lax.rsqrt(jnp.mean(values * values, axis=-1, keepdims=True) + epsilon) * gain


def on_device(
    stream_in, mixer_out, mix_gain, pre_gain, gate_weight, up_weight, gate_scale, up_scale
):
    mixed = stream_in.astype(jnp.float32) + rms_scaled(mixer_out.astype(jnp.float32), mix_gain)
    stream = mixed.astype(jnp.bfloat16)
    normed = rms_scaled(stream.astype(jnp.float32), pre_gain).astype(jnp.bfloat16)
    gate_cast = gate_weight.astype(jnp.bfloat16)
    up_cast = up_weight.astype(jnp.bfloat16)
    gate_full, up_full = in_one_piece((gate_cast, up_cast), "fs", 0, 1)
    piece = lax.all_gather(normed, "tp", axis=0, tiled=True)
    gate = jnp.dot(piece, gate_full, preferred_element_type=jnp.float32) * gate_scale
    up = jnp.dot(piece, up_full, preferred_element_type=jnp.float32) * up_scale
    hidden = (jax.nn.silu(gate) * up).astype(jnp.bfloat16)
    return (hidden, stream)


def solution(mesh):
    return jax.shard_map(
        on_device,
        mesh=mesh,
        in_specs=(
            P(("fs", "tp"), None),
            P(("fs", "tp"), None),
            P(),
            P(),
            P("fs", "tp"),
            P("fs", "tp"),
            P("tp"),
            P("tp"),
        ),
        out_specs=(P("fs", "tp"), P(("fs", "tp"), None)),
        check_vma=False,
    )
```

profile of v0, /device:TPU:1, one launch (start us, length us, event | category | flops | bytes accessed | tf_op | source)
XLA Modules:
  0.0 212.4 jit_solution(17018908718500680703)
XLA Ops:
  7.2 0.0 copy-start.1
  7.2 0.0 copy-start.3
  7.2 0.0 copy-start.2
  7.2 0.0 copy-start.4
  7.2 0.0 all-gather.5.cloned.1.call-start
  7.3 1.2 convert_element_type.29
  8.4 1.0 convert_element_type.30
  9.4 0.8 pad_maximum_fusion
  10.2 0.0 all-gather.5.cloned.1.call-update
  10.3 0.0 all-gather.3.cloned.1.call-start
  10.3 1.5 fusion.6
  11.8 0.0 copy-done.1
  11.8 0.0 copy-done.3
  11.8 0.0 copy-done.2
  11.9 0.0 copy-start.7
  11.9 0.7 fusion.10
  12.6 0.0 copy-start
  12.6 0.0 copy-done.4
  12.7 1.3 fusion.12
  13.9 0.0 all-gather.3.cloned.1.call-update
  14.0 0.0 copy-start.8
  14.0 66.4 %all-gather.5.cloned.1.call-done = bf16[4096,768]{1,0:T(8,128)(2,1)} async-done(((bf16[256,768]{1,0:T(8,128)(2,1)}), bf16[4096,768]{1,0:T(8,128)(2,1)}) %all-gather.5.cloned.1.call-update) | async-done | bytes 6291472 | tf_op jit(solution)/shard_map/all_gather | solution.py:11
  80.4 98.1 %all-gather.3.cloned.1.call-done = bf16[2048,4096]{1,0:T(8,128)(2,1)} async-done(((bf16[128,4096]{1,0:T(8,128)(2,1)}), bf16[2048,4096]{1,0:T(8,128)(2,1)}) %all-gather.3.cloned.1.call-update) | async-done | bytes 16777232 | tf_op jit(solution)/shard_map/all_gather | solution.py:31
  178.5 0.0 copy-done.7
  178.5 0.0 copy-start.5
  178.5 0.0 copy-start.6
  178.5 15.5 %convolution_multiply_fusion.1 = f32[2048,384]{1,0:T(8,128)} fusion(bf16[2048,4096]{1,0:T(8,128)(2,1)} %all-gather.3.cloned.1.call-done, bf16[4096,768]{1,0:T(8,128)(2,1)} %all-gather.5.cloned.1.call-done, f32[384]{0:T(512)S(1)} %copy-done.7), kind=kOutput, calls=%fused_computation.2 | convolution fusion | flops 6443237376 | bytes 23070208 | tf_op jit(solution)/shard_map/dot_general | solution.py:32
  194.0 0.0 copy-done
  194.0 0.0 copy-done.8
  194.0 0.0 copy-done.5
  194.0 0.0 copy-done.6
  194.0 11.5 %fusion.3 = bf16[2048,384]{1,0:T(8,128)(2,1)} fusion(bf16[2048,4096]{1,0:T(8,128)(2,1)S(1)} %copy-done.5, bf16[4096,768]{1,0:T(8,128)(2,1)S(1)} %copy-done.6, f32[2048,384]{1,0:T(8,128)} %convolution_multiply_fusion.1, f32[384]{0:T(512)S(1)} %copy-done.8), kind=kOutput, calls=%fused_computation.5 | convolution fusion | flops 6447955968 | bytes 24643584 | tf_op jit(solution)/shard_map/dot_general | solution.py:33
  (2 shorter events, 0.0 us)
Async XLA Ops:
  7.2 4.7 %copy-start.1 = (bf16[128,4096]{1,0:T(8,128)(2,1)S(1)}, bf16[128,4096]{1,0:T(8,128)(2,1)}, u32[]{:S(2)}) copy-start(bf16[128,4096]{1,0:T(8,128)(2,1)} %param.9) | copy-start | bytes 3145732
  7.2 4.7 %copy-start.3 = (f32[4096]{0:T(1024)S(1)}, f32[4096]{0:T(1024)}, u32[]{:S(2)}) copy-start(f32[4096]{0:T(1024)} %param.10) | copy-start | bytes 49156
  7.2 4.7 %copy-start.2 = (bf16[128,4096]{1,0:T(8,128)(2,1)S(1)}, bf16[128,4096]{1,0:T(8,128)(2,1)}, u32[]{:S(2)}) copy-start(bf16[128,4096]{1,0:T(8,128)(2,1)} %param.8) | copy-start | bytes 3145732
  7.2 5.4 %copy-start.4 = (f32[4096]{0:T(1024)S(1)}, f32[4096]{0:T(1024)}, u32[]{:S(2)}) copy-start(f32[4096]{0:T(1024)} %param.11) | copy-start | bytes 49156
  7.2 73.2 %all-gather.5.cloned.1.call-start = ((), (), s32[]{:S(2)}) async-start(), calls=%async_computation.1 | async-start | bytes 6684672 | tf_op jit(solution)/shard_map/all_gather | solution.py:11
  10.3 168.2 %all-gather.3.cloned.1.call-start = ((), (), s32[]{:S(2)}) async-start(), calls=%async_computation | async-start | bytes 17825792 | tf_op jit(solution)/shard_map/all_gather | solution.py:31
  11.9 166.6 %copy-start.7 = (f32[384]{0:T(512)S(1)}, f32[384]{0:T(512)}, u32[]{:S(2)}) copy-start(f32[384]{0:T(512)} %param.14) | copy-start | bytes 4612
  12.6 181.4 %copy-start = (bf16[128,4096]{1,0:T(8,128)(2,1)}, bf16[128,4096]{1,0:T(8,128)(2,1)S(1)}, u32[]{:S(2)}) copy-start(bf16[128,4096]{1,0:T(8,128)(2,1)S(1)} %get-tuple-element.3) | copy-start | bytes 3145732
  14.0 180.0 %copy-start.8 = (f32[384]{0:T(512)S(1)}, f32[384]{0:T(512)}, u32[]{:S(2)}) copy-start(f32[384]{0:T(512)} %param.15) | copy-start | bytes 4612
  178.5 15.5 %copy-start.5 = (bf16[2048,4096]{1,0:T(8,128)(2,1)S(1)}, bf16[2048,4096]{1,0:T(8,128)(2,1)}, u32[]{:S(2)}) copy-start(bf16[2048,4096]{1,0:T(8,128)(2,1)} %all-gather.3.cloned.1.call-done) | copy-start | bytes 50331652
  178.5 15.5 %copy-start.6 = (bf16[4096,768]{1,0:T(8,128)(2,1)S(1)}, bf16[4096,768]{1,0:T(8,128)(2,1)}, u32[]{:S(2)}) copy-start(bf16[4096,768]{1,0:T(8,128)(2,1)} %all-gather.5.cloned.1.call-done) | copy-start | bytes 18874372
Sparse Core Ops, SparseCore 0:
  10.4 69.8 all-gather.4
  82.8 95.6 all-gather.2
where the time goes:
time: 213 us; the launch traced here: 212 us
  waiting for transfers between devices  165 us (77%)
  matrix products  27 us (13%)
  between operations  14.1 us (7%)
  other arithmetic  6.54 us (3%)
    all_gather x1, waiting for transfers between devices, on_device(): piece = lax.all_gather(normed, 'tp', axis=0, tiled=True)  98.1 us
    all_gather x1, waiting for transfers between devices, in_one_piece(): lax.all_gather(both, axis, axis=dim, tiled=True)  66.4 us
    dot_general x1, matrix products, on_device(): jnp.dot(piece, gate_full, preferred_element_type=jnp.float32) * gate_scale  15.5 us
    dot_general x1, matrix products, on_device(): up = jnp.dot(piece, up_full, preferred_element_type=jnp.float32) * up_scale  11.5 us
  transfers between devices with their start and end apart: 2, of which 2 were waited for; matrix products, arithmetic and copies ran while one was open for 2% of the time, Pallas kernels for 0%

commit v1 on v0

v1 whole, which is shorter than its diff:
```python
import functools

import jax
import jax.numpy as jnp
from jax import lax
from jax.experimental import pallas as pl
from jax.experimental.pallas import tpu as pltpu
from jax.sharding import PartitionSpec as P

MESH = pl.DeviceIdType.MESH
epsilon = 1e-06

D = 4096
ROWS = 128
COLS = 384
SIDE = 4
DEEP = 8
SHARD = 256
HALF = SHARD // 2
QUARTER = HALF // 2
CHUNK = 32
CHUNKS = ROWS // CHUNK
LANES = 512
TILES = COLS // 128
F32 = jnp.float32
BF16 = jnp.bfloat16


def kernel(
    stream_in, mixer_out, mix_gain, pre_gain, gate_w, up_w, gate_s, up_s,
    hidden, stream,
    tok, w, stream_v, mixer_v, stream_o, gate_v, up_v, mg, pg, gs, us, hid,
    in_sem, out_sem, zs, zr, ds_, dr, ws, wr,
):
    fs, tp = lax.axis_index("fs"), lax.axis_index("tp")
    x, y = lax.rem(fs, SIDE), lax.div(fs, SIDE)
    core, z = lax.rem(tp, 2), lax.div(tp, 2)

    def up_by(v, k, n):
        return lax.rem(v + k, n)

    along_z = {s: (fs, up_by(z, k, DEEP) * 2 + core) for s, k in ((0, 1), (1, DEEP - 1))}
    partner = (fs, z * 2 + (1 - core))
    along = {
        ("x", 0): (y * SIDE + up_by(x, 1, SIDE), tp),
        ("x", 1): (y * SIDE + up_by(x, SIDE - 1, SIDE), tp),
        ("y", 0): (up_by(y, 1, SIDE) * SIDE + x, tp),
        ("y", 1): (up_by(y, SIDE - 1, SIDE) * SIDE + x, tp),
    }
    neighbours = list(along_z.values()) + [partner] + list(along.values())

    loads = {}

    def load(name, src, dst):
        c = pltpu.make_async_copy(src, dst, in_sem.at[len(loads)])
        c.start()
        loads[name] = c

    load("mg", mix_gain, mg)
    load("pg", pre_gain, pg)
    for c in range(CHUNKS):
        rows = pl.ds(c * CHUNK, CHUNK)
        load(("m", c), mixer_out.at[rows], mixer_v.at[rows])
        load(("s", c), stream_in.at[rows], stream_v.at[rows])
        if c == 0:
            load("gw", gate_w, gate_v)
            load("uw", up_w, up_v)
    load("gs", gate_s, gs)
    load("us", up_s, us)

    barrier = pltpu.get_barrier_semaphore()
    for n in neighbours:
        pl.semaphore_signal(barrier, inc=1, device_id=n, device_id_type=MESH)

    def norm(c):
        loads[("m", c)].wait()
        loads[("s", c)].wait()

        def some(i, carry):
            rows = pl.ds(pl.multiple_of(c * CHUNK + i * 16, 16), 16)
            parts = [pl.ds(k * LANES, LANES) for k in range(D // LANES)]
            total = jnp.zeros((16, LANES), F32)
            for p in parts:
                m = mixer_v[rows, p].astype(F32)
                total += m * m
            inv = lax.rsqrt(jnp.sum(total, axis=-1, keepdims=True) * (1.0 / D) + epsilon)
            total = jnp.zeros((16, LANES), F32)
            for p in parts:
                m = mixer_v[rows, p].astype(F32)
                s = (stream_v[rows, p].astype(F32) + m * inv * mg[:, p]).astype(BF16)
                stream_o[rows, p] = s
                s = s.astype(F32)
                total += s * s
            inv = lax.rsqrt(jnp.sum(total, axis=-1, keepdims=True) * (1.0 / D) + epsilon)
            for p in parts:
                s = stream_o[rows, p].astype(F32)
                tok[0, rows, p] = (s * inv * pg[:, p]).astype(BF16)
            return carry

        lax.fori_loop(0, CHUNK // 16, some, 0)

    sent = []

    def send(src, dst, ssem, rsem, device):
        c = pltpu.make_async_remote_copy(
            src_ref=src, dst_ref=dst, send_sem=ssem, recv_sem=rsem,
            device_id=device, device_id_type=MESH,
        )
        c.start()
        sent.append(c)

    def arrived(dst, ssem, rsem):
        pltpu.make_async_remote_copy(
            src_ref=dst, dst_ref=dst, send_sem=ssem, recv_sem=rsem,
            device_id=partner, device_id_type=MESH,
        ).wait_recv()

    def piece(dz, which, c):
        return tok.at[dz, pl.ds(which * ROWS + c * CHUNK, CHUNK)]

    def z_index(dz, c):
        return (dz - 1) * CHUNKS + c

    def z_send(way, dz, c):
        if dz >= DEEP // 2 or (dz == DEEP // 2 - 1 and (c < CHUNKS // 2) == (way == 1)):
            return
        here, there = (dz, dz + 1) if way == 0 else (-dz % DEEP, DEEP - 1 - dz)
        i = z_index(dz + 1, c)
        send(piece(here, 0, c), piece(there, 0, c), zs.at[way, i], zr.at[way, i], along_z[way])

    def d_send(dz, c):
        i = dz * CHUNKS + c
        send(piece(dz, 0, c), piece(dz, 1, c), ds_.at[i], dr.at[i], partner)

    def z_take(way, steps, c):
        i = z_index(steps, c)
        dz = steps if way == 0 else DEEP - steps
        arrived(piece(dz, 0, c), zs.at[way, i], zr.at[way, i])
        z_send(way, steps, c)
        d_send(dz, c)

    def d_take(dz, c):
        i = dz * CHUNKS + c
        arrived(piece(dz, 1, c), ds_.at[i], dr.at[i])

    rings = {"A": ("x", 0, 0, 0), "B": ("y", 0, 1, 1)}
    for j in range(SIDE):
        rings[("A", j)] = ("y", j, 0, 2 + j)
        rings[("B", j)] = ("x", j, 1, 2 + SIDE + j)

    def w_rows(ring, step, start, count):
        axis, j, half, _ = rings[ring]
        dx, dy = (step, j) if axis == "x" else (j, step)
        owner = up_by(y, SIDE - dy, SIDE) * SIDE + up_by(x, SIDE - dx, SIDE)
        return w.at[pl.ds(pl.multiple_of(owner * SHARD + half * HALF + start, QUARTER), count)]

    def w_send(ring, step, start, count, way, i):
        axis, _, _, r = rings[ring]
        ref = w_rows(ring, step, start, count)
        send(ref, ref, ws.at[r, i], wr.at[r, i], along[(axis, way)])

    def w_begin(ring):
        w_send(ring, 0, 0, HALF, 0, 0)
        w_send(ring, 0, 0, HALF, 1, 1)

    def w_near(ring):
        r = rings[ring][3]
        arrived(w_rows(ring, 1, 0, HALF), ws.at[r, 0], wr.at[r, 0])
        w_send(ring, 1, 0, QUARTER, 0, 2)
        arrived(w_rows(ring, SIDE - 1, 0, HALF), ws.at[r, 1], wr.at[r, 1])
        w_send(ring, SIDE - 1, QUARTER, QUARTER, 1, 3)

    def w_far(ring):
        r = rings[ring][3]
        arrived(w_rows(ring, 2, 0, QUARTER), ws.at[r, 2], wr.at[r, 2])
        arrived(w_rows(ring, 2, QUARTER, QUARTER), ws.at[r, 3], wr.at[r, 3])

    outs = []

    def row_of(dz, which):
        owner = up_by(z, DEEP - dz, DEEP) * 2 + (core if which == 0 else 1 - core)
        return owner * ROWS

    def project(dz, spans):
        def tile(j, carry):
            cols = pl.ds(pl.multiple_of(j * 256, 256), 256)
            mine = pl.ds(pl.multiple_of(j * 128, 128), 128)
            parts = [tok[dz, pl.ds(a, n), :] for a, n in spans]
            lhs = parts[0] if len(parts) == 1 else jnp.concatenate(parts, axis=0)
            both = jnp.dot(lhs, w[:, cols], preferred_element_type=F32)
            gate = both[:, :128] * gs[:, mine]
            up = both[:, 128:] * us[:, mine]
            out = (gate / (1.0 + jnp.exp(-gate)) * up).astype(BF16)
            at = 0
            for a, n in spans:
                hid[dz, pl.ds(a, n), mine] = out[at:at + n]
                at += n
            return carry

        lax.fori_loop(0, TILES, tile, 0)
        for a, n in spans:
            first = a
            while first < a + n:
                which = first // ROWS
                size = min(a + n, (which + 1) * ROWS) - first
                to = pl.multiple_of(row_of(dz, which) + first % ROWS, CHUNK)
                c = pltpu.make_async_copy(
                    hid.at[dz, pl.ds(first, size)],
                    hidden.at[pl.ds(to, size)],
                    out_sem.at[len(outs)],
                )
                c.start()
                outs.append(c)
                first += size

    loads["mg"].wait()
    loads["pg"].wait()
    loads["gw"].wait()
    loads["uw"].wait()
    own = pl.ds(pl.multiple_of(fs * SHARD, SHARD), SHARD)
    for j in range(TILES):
        w[own, j * 256:j * 256 + 128] = gate_v[:, j * 128:(j + 1) * 128].astype(BF16)
        w[own, j * 256 + 128:(j + 1) * 256] = up_v[:, j * 128:(j + 1) * 128].astype(BF16)

    def own_out(c):
        z_send(0, 0, c)
        z_send(1, 0, c)
        d_send(0, c)

    norm(0)
    pl.semaphore_wait(barrier, len(neighbours))
    w_begin("A")
    w_begin("B")
    w_begin(("A", 0))
    w_begin(("B", 0))
    for c in range(1, CHUNKS):
        norm(c)
        own_out(c - 1)
    loads["gs"].wait()
    loads["us"].wait()
    c = pltpu.make_async_copy(stream_o, stream, out_sem.at[0])
    c.start()
    outs.append(c)
    own_out(CHUNKS - 1)

    def z_both(steps, c):
        z_take(0, steps, c)
        z_take(1, steps, c)

    w_near("A")
    w_near("B")
    for r in ("A", "B"):
        w_begin((r, 1))
        w_begin((r, 3))
    z_both(1, 0)
    w_near(("A", 0))
    w_near(("B", 0))
    w_far("A")
    w_far("B")
    w_begin(("A", 2))
    w_begin(("B", 2))
    z_both(1, 1)
    w_near(("A", 1))
    w_near(("B", 1))
    z_both(1, 2)
    w_near(("A", 3))
    w_near(("B", 3))
    w_far(("A", 0))
    w_far(("B", 0))
    z_both(1, 3)
    w_near(("A", 2))
    w_near(("B", 2))
    for j in (1, 3):
        w_far(("A", j))
        w_far(("B", j))
    z_both(2, 0)
    w_far(("A", 2))
    w_far(("B", 2))

    def whole(dz):
        for c in range(CHUNKS):
            d_take(dz, c)
        project(dz, ((0, 2 * ROWS),))

    whole(0)
    whole(1)
    z_both(2, 1)
    whole(DEEP - 1)
    z_both(2, 2)
    z_both(2, 3)
    whole(2)
    z_both(3, 0)
    whole(DEEP - 2)
    z_both(3, 1)
    z_both(3, 2)
    z_both(3, 3)
    whole(3)
    whole(DEEP - 3)
    far = DEEP // 2
    for c in range(CHUNKS // 2):
        cs = (c, c + CHUNKS // 2)
        z_take(0, far, cs[0])
        z_take(1, far, cs[1])
        for k in cs:
            d_take(far, k)
        project(far, tuple((h * ROWS + k * CHUNK, CHUNK) for h in (0, 1) for k in cs))

    for c in sent:
        c.wait_send()
    for c in outs:
        c.wait()


def on_device(
    stream_in, mixer_out, mix_gain, pre_gain, gate_weight, up_weight, gate_scale, up_scale
):
    any_ = pl.BlockSpec(memory_space=pltpu.HBM)
    dma = pltpu.SemaphoreType.DMA
    z_copies = (DEEP // 2) * CHUNKS
    return pl.pallas_call(
        kernel,
        name="gathered_projections",
        out_shape=(
            jax.ShapeDtypeStruct((DEEP * 2 * ROWS, COLS), BF16),
            jax.ShapeDtypeStruct((ROWS, D), BF16),
        ),
        in_specs=[any_] * 8,
        out_specs=(any_, any_),
        scratch_shapes=[
            pltpu.VMEM((DEEP, 2 * ROWS, D), BF16),
            pltpu.VMEM((D, 2 * COLS), BF16),
            pltpu.VMEM((ROWS, D), BF16),
            pltpu.VMEM((ROWS, D), BF16),
            pltpu.VMEM((ROWS, D), BF16),
            pltpu.VMEM((SHARD, COLS), F32),
            pltpu.VMEM((SHARD, COLS), F32),
            pltpu.VMEM((1, D), F32),
            pltpu.VMEM((1, D), F32),
            pltpu.VMEM((1, COLS), F32),
            pltpu.VMEM((1, COLS), F32),
            pltpu.VMEM((DEEP, 2 * ROWS, COLS), BF16),
            dma((6 + 2 * CHUNKS,)),
            dma((64,)),
            dma((2, z_copies)),
            dma((2, z_copies)),
            dma((DEEP * CHUNKS,)),
            dma((DEEP * CHUNKS,)),
            dma((2 + 2 * SIDE, 4)),
            dma((2 + 2 * SIDE, 4)),
        ],
        compiler_params=pltpu.CompilerParams(
            collective_id=0, has_side_effects=True, vmem_limit_bytes=56 * 2**20
        ),
    )(
        stream_in, mixer_out, mix_gain.reshape(1, -1), pre_gain.reshape(1, -1),
        gate_weight, up_weight, gate_scale.reshape(1, -1), up_scale.reshape(1, -1),
    )


def solution(mesh):
    return jax.shard_map(
        on_device,
        mesh=mesh,
        in_specs=(
            P(("fs", "tp"), None),
            P(("fs", "tp"), None),
            P(),
            P(),
            P("fs", "tp"),
            P("fs", "tp"),
            P("tp"),
            P("tp"),
        ),
        out_specs=(P("fs", "tp"), P(("fs", "tp"), None)),
        check_vma=False,
    )
```

time: 213 us -> 103 us (0.48)
  waiting for transfers between devices: 165 us -> 0 us
  Pallas kernels: 0 us -> 96.1 us
  matrix products: 27 us -> 0 us
  between operations: 14.1 us -> 0.65 us
  other arithmetic: 6.54 us -> 0 us
  local copies, waits for them, and re-layouts: 0.05 us -> 6.26 us
    all_gather x2 -> x0, waiting for transfers between devices: 164 us -> none  [the longest x1 98.1 us: on_device(): piece = lax.all_gather(normed, 'tp', axis=0, tiled=True)]
    pallas_call x0 -> x1, Pallas kernels: none -> 96.1 us  [on_device(): pl.pallas_call(kernel, name='gathered_projections', out_shape=(jax.ShapeD...]
    dot_general x2 -> x0, matrix products: 27 us -> none  [the longest x1 15.5 us: on_device(): jnp.dot(piece, gate_full, preferred_element_type=jnp.float32) * gate_scale]
    unnamed x18 -> x4, local copies, waits for them, and re-layouts: 0.05 us -> 3.77 us
    convert_element_type x3 -> x0, other arithmetic: 3.47 us -> none  [the longest x1 1.3 us: on_device(): rms_scaled(stream.astype(jnp.float32), pre_gain).astype(jnp.bfloat16)]
    reshape x0 -> x2, local copies, waits for them, and re-layouts: none -> 2.49 us  [the longest x1 1.25 us: on_device(): gate_scale.reshape(1, -1)]
    reduce_sum x2 -> x0, other arithmetic: 2.26 us -> none  [rms_scaled(): jnp.mean(values * values, axis=-1, keepdims=True) + epsilon]
  transfers between devices with their start and end apart: 2 -> 0, of which waited for: 2 -> 0; matrix products, arithmetic and copies ran while one was open for 2% -> 0% of each run, Pallas kernels for 0% -> 0%
where the time goes in v1:
time: 103 us
  Pallas kernels  96.1 us (93%)
  local copies, waits for them, and re-layouts  6.26 us (6%)
    pallas_call x1, Pallas kernels, on_device(): pl.pallas_call(kernel, name='gathered_projections', out_shape=(jax.ShapeD...  96.1 us
    unnamed x4, local copies, waits for them, and re-layouts  3.77 us

profile of v1, /device:TPU:1, one launch (start us, length us, event | category | flops | bytes accessed | tf_op | source)
XLA Modules:
  0.0 103.0 jit_solution(6517379503701248270)
XLA Ops:
  0.6 1.2 %reshape.18.gate_s = f32[1,384]{1,0:T(1,128)} reshape(f32[384]{0:T(512)} %param.14) | data formatting | bytes 3072 | tf_op jit(solution)/shard_map/reshape | solution.py:356
  1.9 1.2 %reshape.19.up_s = f32[1,384]{1,0:T(1,128)} reshape(f32[384]{0:T(512)} %param.15) | data formatting | bytes 3072 | tf_op jit(solution)/shard_map/reshape | solution.py:356
  3.1 96.1 %gathered_projections.1 = (bf16[2048,384]{1,0:T(8,128)(2,1)}, bf16[128,4096]{1,0:T(8,128)(2,1)}) custom-call(bf16[128,4096]{1,0:T(8,128)(2,1)} %stream_in.1, bf16[128,4096]{1,0:T(8,128)(2,1)} %mixer_out.1, f32[1,4096]{1,0:T(1,128)} %bitcast.2, f32[1,4096]{1,0:T(1,128)} %bitcast.3, f32[256,384]{1,0:T(8,128)} %gate_w.1, f32[256,384]{1,0:T(8,128)} %up_w.1, ...), custom_call_target="tpu_custom_call" | custom-call | tf_op jit(solution)/shard_map/gathered_projections/pallas_call | solution.py:320
  99.2 0.0 copy-start
  99.2 2.8 %copy.12 = bf16[2048,384]{1,0:T(8,128)(2,1)} copy(bf16[2048,384]{1,0:T(8,128)(2,1)} %get-tuple-element.4) | data formatting | bytes 3145728
  102.0 0.0 copy-done
  102.0 1.0 copy.13
Async XLA Ops:
  99.2 2.8 %copy-start = (bf16[128,4096]{1,0:T(8,128)(2,1)S(1)}, bf16[128,4096]{1,0:T(8,128)(2,1)}, u32[]{:S(2)}) copy-start(bf16[128,4096]{1,0:T(8,128)(2,1)} %get-tuple-element.5) | copy-start | bytes 3145732

commit v2 on v1

--- a/solution.py
+++ b/solution.py
@@ -20,6 +20,7 @@
 QUARTER = HALF // 2
 CHUNK = 32
 CHUNKS = ROWS // CHUNK
+FAR = ((0, 32), (32, 16), (48, 16))
 LANES = 512
 TILES = COLS // 128
 F32 = jnp.float32
@@ -29,8 +30,8 @@
 def kernel(
     stream_in, mixer_out, mix_gain, pre_gain, gate_w, up_w, gate_s, up_s,
     hidden, stream,
-    tok, w, stream_v, mixer_v, stream_o, gate_v, up_v, mg, pg, gs, us, hid,
-    in_sem, out_sem, zs, zr, ds_, dr, ws, wr,
+    tok, w, stream_v, mixer_v, gate_v, up_v, mg, pg, gs, us, scales,
+    in_sem, zs, zr, ds_, dr, ws, wr,
 ):
     fs, tp = lax.axis_index("fs"), lax.axis_index("tp")
     x, y = lax.rem(fs, SIDE), lax.div(fs, SIDE)
@@ -88,12 +89,12 @@
             for p in parts:
                 m = mixer_v[rows, p].astype(F32)
                 s = (stream_v[rows, p].astype(F32) + m * inv * mg[:, p]).astype(BF16)
-                stream_o[rows, p] = s
+                stream[rows, p] = s
                 s = s.astype(F32)
                 total += s * s
             inv = lax.rsqrt(jnp.sum(total, axis=-1, keepdims=True) * (1.0 / D) + epsilon)
             for p in parts:
-                s = stream_o[rows, p].astype(F32)
+                s = stream[rows, p].astype(F32)
                 tok[0, rows, p] = (s * inv * pg[:, p]).astype(BF16)
             return carry
 
@@ -115,33 +116,55 @@
             device_id=partner, device_id_type=MESH,
         ).wait_recv()
 
-    def piece(dz, which, c):
-        return tok.at[dz, pl.ds(which * ROWS + c * CHUNK, CHUNK)]
-
-    def z_index(dz, c):
-        return (dz - 1) * CHUNKS + c
-
-    def z_send(way, dz, c):
-        if dz >= DEEP // 2 or (dz == DEEP // 2 - 1 and (c < CHUNKS // 2) == (way == 1)):
-            return
-        here, there = (dz, dz + 1) if way == 0 else (-dz % DEEP, DEEP - 1 - dz)
-        i = z_index(dz + 1, c)
-        send(piece(here, 0, c), piece(there, 0, c), zs.at[way, i], zr.at[way, i], along_z[way])
-
-    def d_send(dz, c):
-        i = dz * CHUNKS + c
-        send(piece(dz, 0, c), piece(dz, 1, c), ds_.at[i], dr.at[i], partner)
+    far = DEEP // 2
+
+    def piece(dz, which, rows):
+        return tok.at[dz, pl.ds(which * ROWS + rows[0], rows[1])]
+
+    def chunk(c):
+        return (c * CHUNK, CHUNK)
+
+    def far_piece(way, k):
+        return (way * (ROWS // 2) + FAR[k][0], FAR[k][1])
+
+    def z_send(way, steps, rows, i):
+        here, there = (steps, steps + 1) if way == 0 else (-steps % DEEP, DEEP - 1 - steps)
+        send(piece(here, 0, rows), piece(there, 0, rows), zs.at[way, i], zr.at[way, i], along_z[way])
+
+    def z_forward(way, steps, c):
+        if steps < far - 1:
+            z_send(way, steps, chunk(c), steps * CHUNKS + c)
+        elif c // (CHUNKS // 2) == way:
+            first = c % (CHUNKS // 2) * CHUNK
+            for k, (start, _) in enumerate(FAR):
+                if first <= start < first + CHUNK:
+                    z_send(way, steps, far_piece(way, k), steps * CHUNKS + k)
+
+    def d_send(dz, rows, i):
+        send(piece(dz, 0, rows), piece(dz, 1, rows), ds_.at[i], dr.at[i], partner)
+
+    def z_arrived(way, steps, rows, i):
+        dz = steps if way == 0 else DEEP - steps
+        arrived(piece(dz, 0, rows), zs.at[way, i], zr.at[way, i])
+        return dz
 
     def z_take(way, steps, c):
-        i = z_index(steps, c)
-        dz = steps if way == 0 else DEEP - steps
-        arrived(piece(dz, 0, c), zs.at[way, i], zr.at[way, i])
-        z_send(way, steps, c)
-        d_send(dz, c)
-
-    def d_take(dz, c):
-        i = dz * CHUNKS + c
-        arrived(piece(dz, 1, c), ds_.at[i], dr.at[i])
+        dz = z_arrived(way, steps, chunk(c), (steps - 1) * CHUNKS + c)
+        z_forward(way, steps, c)
+        d_send(dz, chunk(c), dz * CHUNKS + c)
+
+    def d_take(dz, rows, i):
+        arrived(piece(dz, 1, rows), ds_.at[i], dr.at[i])
+
+    def far_index(way, k):
+        return DEEP * CHUNKS + way * len(FAR) + k
+
+    def far_take(k):
+        for way in (0, 1):
+            z_arrived(way, far, far_piece(way, k), (far - 1) * CHUNKS + k)
+            d_send(far, far_piece(way, k), far_index(way, k))
+        for way in (0, 1):
+            d_take(far, far_piece(way, k), far_index(way, k))
 
     rings = {"A": ("x", 0, 0, 0), "B": ("y", 0, 1, 1)}
     for j in range(SIDE):
@@ -174,8 +197,6 @@
         r = rings[ring][3]
         arrived(w_rows(ring, 2, 0, QUARTER), ws.at[r, 2], wr.at[r, 2])
         arrived(w_rows(ring, 2, QUARTER, QUARTER), ws.at[r, 3], wr.at[r, 3])
-
-    outs = []
 
     def row_of(dz, which):
         owner = up_by(z, DEEP - dz, DEEP) * 2 + (core if which == 0 else 1 - core)
@@ -188,33 +209,29 @@
             parts = [tok[dz, pl.ds(a, n), :] for a, n in spans]
             lhs = parts[0] if len(parts) == 1 else jnp.concatenate(parts, axis=0)
             both = jnp.dot(lhs, w[:, cols], preferred_element_type=F32)
-            gate = both[:, :128] * gs[:, mine]
-            up = both[:, 128:] * us[:, mine]
+            gate = both[:, :128] * scales[j, 0:1]
+            up = both[:, 128:] * scales[j, 1:2]
             out = (gate / (1.0 + jnp.exp(-gate)) * up).astype(BF16)
             at = 0
             for a, n in spans:
-                hid[dz, pl.ds(a, n), mine] = out[at:at + n]
-                at += n
+                while n > 0:
+                    size = min(n, ROWS - a % ROWS)
+                    to = pl.multiple_of(row_of(dz, a // ROWS) + a % ROWS, 16)
+                    hidden[pl.ds(to, size), mine] = out[at:at + size]
+                    a, n, at = a + size, n - size, at + size
             return carry
 
         lax.fori_loop(0, TILES, tile, 0)
-        for a, n in spans:
-            first = a
-            while first < a + n:
-                which = first // ROWS
-                size = min(a + n, (which + 1) * ROWS) - first
-                to = pl.multiple_of(row_of(dz, which) + first % ROWS, CHUNK)
-                c = pltpu.make_async_copy(
-                    hid.at[dz, pl.ds(first, size)],
-                    hidden.at[pl.ds(to, size)],
-                    out_sem.at[len(outs)],
-                )
-                c.start()
-                outs.append(c)
-                first += size
+
+    def own_out(c):
+        z_forward(0, 0, c)
+        z_forward(1, 0, c)
+        d_send(0, chunk(c), c)
 
     loads["mg"].wait()
     loads["pg"].wait()
+    norm(0)
+    pl.semaphore_wait(barrier, len(neighbours))
     loads["gw"].wait()
     loads["uw"].wait()
     own = pl.ds(pl.multiple_of(fs * SHARD, SHARD), SHARD)
@@ -222,25 +239,18 @@
         w[own, j * 256:j * 256 + 128] = gate_v[:, j * 128:(j + 1) * 128].astype(BF16)
         w[own, j * 256 + 128:(j + 1) * 256] = up_v[:, j * 128:(j + 1) * 128].astype(BF16)
 
-    def own_out(c):
-        z_send(0, 0, c)
-        z_send(1, 0, c)
-        d_send(0, c)
-
-    norm(0)
-    pl.semaphore_wait(barrier, len(neighbours))
-    w_begin("A")
-    w_begin("B")
-    w_begin(("A", 0))
-    w_begin(("B", 0))
-    for c in range(1, CHUNKS):
+    own_out(0)
+    norm(1)
+    for r in ("A", "B", ("A", 0), ("B", 0)):
+        w_begin(r)
+    for c in range(2, CHUNKS):
         norm(c)
         own_out(c - 1)
     loads["gs"].wait()
     loads["us"].wait()
-    c = pltpu.make_async_copy(stream_o, stream, out_sem.at[0])
-    c.start()
-    outs.append(c)
+    for j in range(TILES):
+        scales[j, 0] = gs[j * 128:(j + 1) * 128]
+        scales[j, 1] = us[j * 128:(j + 1) * 128]
     own_out(CHUNKS - 1)
 
     def z_both(steps, c):
@@ -279,7 +289,7 @@
 
     def whole(dz):
         for c in range(CHUNKS):
-            d_take(dz, c)
+            d_take(dz, chunk(c), dz * CHUNKS + c)
         project(dz, ((0, 2 * ROWS),))
 
     whole(0)
@@ -296,19 +306,15 @@
     z_both(3, 3)
     whole(3)
     whole(DEEP - 3)
-    far = DEEP // 2
-    for c in range(CHUNKS // 2):
-        cs = (c, c + CHUNKS // 2)
-        z_take(0, far, cs[0])
-        z_take(1, far, cs[1])
-        for k in cs:
-            d_take(far, k)
-        project(far, tuple((h * ROWS + k * CHUNK, CHUNK) for h in (0, 1) for k in cs))
+    for k in range(len(FAR)):
+        far_take(k)
+        project(far, tuple(
+            (which * ROWS + rows[0], rows[1])
+            for which in (0, 1) for rows in (far_piece(0, k), far_piece(1, k))
+        ))
 
     for c in sent:
         c.wait_send()
-    for c in outs:
-        c.wait()
 
 
 def on_device(
@@ -325,36 +331,37 @@
             jax.ShapeDtypeStruct((ROWS, D), BF16),
         ),
         in_specs=[any_] * 8,
-        out_specs=(any_, any_),
+        out_specs=(pl.BlockSpec(memory_space=pltpu.VMEM),) * 2,
         scratch_shapes=[
             pltpu.VMEM((DEEP, 2 * ROWS, D), BF16),
             pltpu.VMEM((D, 2 * COLS), BF16),
-            pltpu.VMEM((ROWS, D), BF16),
             pltpu.VMEM((ROWS, D), BF16),
             pltpu.VMEM((ROWS, D), BF16),
             pltpu.VMEM((SHARD, COLS), F32),
             pltpu.VMEM((SHARD, COLS), F32),
             pltpu.VMEM((1, D), F32),
             pltpu.VMEM((1, D), F32),
-            pltpu.VMEM((1, COLS), F32),
-            pltpu.VMEM((1, COLS), F32),
-            pltpu.VMEM((DEEP, 2 * ROWS, COLS), BF16),
+            pltpu.VMEM((COLS,), F32),
+            pltpu.VMEM((COLS,), F32),
+            pltpu.VMEM((TILES, 2, 128), F32),
             dma((6 + 2 * CHUNKS,)),
-            dma((64,)),
             dma((2, z_copies)),
             dma((2, z_copies)),
-            dma((DEEP * CHUNKS,)),
-            dma((DEEP * CHUNKS,)),
+            dma((DEEP * CHUNKS + 2 * len(FAR),)),
+            dma((DEEP * CHUNKS + 2 * len(FAR),)),
             dma((2 + 2 * SIDE, 4)),
             dma((2 + 2 * SIDE, 4)),
         ],
         compiler_params=pltpu.CompilerParams(
-            collective_id=0, has_side_effects=True, vmem_limit_bytes=56 * 2**20
+            collective_id=0, has_side_effects=True, vmem_limit_bytes=40 * 2**20
         ),
-    )(
-        stream_in, mixer_out, mix_gain.reshape(1, -1), pre_gain.reshape(1, -1),
-        gate_weight, up_weight, gate_scale.reshape(1, -1), up_scale.reshape(1, -1),
-    )
+    )(*(
+        pltpu.with_memory_space_constraint(a, pltpu.HBM)
+        for a in (
+            stream_in, mixer_out, mix_gain.reshape(1, -1), pre_gain.reshape(1, -1),
+            gate_weight, up_weight, gate_scale, up_scale,
+        )
+    ))
 
 
 def solution(mesh):

time: 103 us -> 98.9 us (0.960)
  local copies, waits for them, and re-layouts: 6.26 us -> 2.11 us
    reshape x2 -> x0, local copies, waits for them, and re-layouts: 2.49 us -> none  [the longest x1 1.25 us: on_device(): gate_scale.reshape(1, -1)]
    unnamed x4 -> x2, local copies, waits for them, and re-layouts: 3.77 us -> 2.11 us
where the time goes in v2:
time: 98.9 us; the launch traced here: 98.7 us
  Pallas kernels  95.9 us (97%)
  local copies, waits for them, and re-layouts  2.11 us (2%)
    pallas_call x1, Pallas kernels, on_device(): pl.pallas_call(kernel, name='gathered_projections', out_shape=(jax.ShapeD...  95.9 us
    unnamed x2, local copies, waits for them, and re-layouts  2.11 us

profile of v2, /device:TPU:1, one launch (start us, length us, event | category | flops | bytes accessed | tf_op | source)
XLA Modules:
  0.0 98.7 jit_solution(15513251655707099076)
XLA Ops:
  0.6 95.9 %gathered_projections.1 = (bf16[2048,384]{1,0:T(8,128)(2,1)S(1)}, bf16[128,4096]{1,0:T(8,128)(2,1)S(1)}) custom-call(bf16[128,4096]{1,0:T(8,128)(2,1)} %stream_in.1, bf16[128,4096]{1,0:T(8,128)(2,1)} %mixer_out.1, f32[1,4096]{1,0:T(1,128)} %bitcast.2, f32[1,4096]{1,0:T(1,128)} %bitcast.3, f32[256,384]{1,0:T(8,128)} %gate_w.1, f32[256,384]{1,0:T(8,128)} %up_w.1, ...), custom_call_target="tpu_custom_call" | custom-call | tf_op jit(solution)/shard_map/gathered_projections/pallas_call | solution.py:326
  96.6 1.1 %copy.12 = bf16[2048,384]{1,0:T(8,128)(2,1)} copy(bf16[2048,384]{1,0:T(8,128)(2,1)S(1)} %get-tuple-element.4) | data formatting | bytes 3145728
  97.7 1.0 copy.13

commit v3 on v2

v3 whole, which is shorter than its diff:
```python
import functools

import jax
import jax.numpy as jnp
from jax import lax
from jax.experimental import pallas as pl
from jax.experimental.pallas import tpu as pltpu
from jax.sharding import PartitionSpec as P

MESH = pl.DeviceIdType.MESH
epsilon = 1e-06

D = 4096
ROWS = 128
COLS = 384
SIDE = 4
DEEP = 8
SHARD = 256
HALF = SHARD // 2
QUARTER = HALF // 2
CHUNK = 32
CHUNKS = ROWS // CHUNK
WINDOW = DEEP // 2
WHOLE = tuple((c * CHUNK, CHUNK) for c in range(CHUNKS))
LAST = WHOLE[:-1] + ((96, 16), (112, 16))
LANES = 512
TILES = COLS // 128
F32 = jnp.float32
BF16 = jnp.bfloat16


def kernel(
    stream_in, mixer_out, mix_gain, pre_gain, gate_w, up_w, gate_s, up_s,
    hidden, stream,
    tok, transit, w0, w1, stream_v, mixer_v, gate_v, up_v, mg, pg, gs, us, gs1, us1,
    scales, given,
    in_sem, os_, or_, ts, tr, ds_, dr, xs, xr, rs, rr, ws, wr,
):
    fs, tp = lax.axis_index("fs"), lax.axis_index("tp")
    x, y = lax.rem(fs, SIDE), lax.div(fs, SIDE)
    core, z = lax.rem(tp, 2), lax.div(tp, 2)
    side = 1 - 2 * lax.rem(z, 2)

    def up_by(v, k, n):
        return lax.rem(v + k, n)

    def chip(k):
        return lax.rem(z + k * side + 2 * DEEP, DEEP)

    other = (fs, z * 2 + (1 - core))
    mate = (fs, chip(1) * 2 + core)
    outer = (fs, chip(-1) * 2 + core)
    along = {
        ("x", 0): (y * SIDE + up_by(x, 1, SIDE), tp),
        ("x", 1): (y * SIDE + up_by(x, SIDE - 1, SIDE), tp),
        ("y", 0): (up_by(y, 1, SIDE) * SIDE + x, tp),
        ("y", 1): (up_by(y, SIDE - 1, SIDE) * SIDE + x, tp),
    }
    neighbours = [mate, outer, other] + list(along.values())

    loads = {}

    def load(name, src, dst):
        c = pltpu.make_async_copy(src, dst, in_sem.at[len(loads)])
        c.start()
        loads[name] = c

    load("gw", gate_w, gate_v)
    load("uw", up_w, up_v)
    load("mg", mix_gain, mg)
    load("pg", pre_gain, pg)
    for c in range(CHUNKS):
        rows = pl.ds(c * CHUNK, CHUNK)
        load(("m", c), mixer_out.at[rows], mixer_v.at[rows])
        load(("s", c), stream_in.at[rows], stream_v.at[rows])
    load("gs", gate_s, gs)
    load("us", up_s, us)

    barrier = pltpu.get_barrier_semaphore()
    for n in neighbours:
        pl.semaphore_signal(barrier, inc=1, device_id=n, device_id_type=MESH)

    def norm(c):
        loads[("m", c)].wait()
        loads[("s", c)].wait()

        def some(i, carry):
            rows = pl.ds(pl.multiple_of(c * CHUNK + i * 16, 16), 16)
            parts = [pl.ds(k * LANES, LANES) for k in range(D // LANES)]
            total = jnp.zeros((16, LANES), F32)
            for p in parts:
                m = mixer_v[rows, p].astype(F32)
                total += m * m
            inv = lax.rsqrt(jnp.sum(total, axis=-1, keepdims=True) * (1.0 / D) + epsilon)
            total = jnp.zeros((16, LANES), F32)
            for p in parts:
                m = mixer_v[rows, p].astype(F32)
                s = (stream_v[rows, p].astype(F32) + m * inv * mg[:, p]).astype(BF16)
                stream[rows, p] = s
                s = s.astype(F32)
                total += s * s
            inv = lax.rsqrt(jnp.sum(total, axis=-1, keepdims=True) * (1.0 / D) + epsilon)
            for p in parts:
                s = stream[rows, p].astype(F32)
                tok[0, rows, p] = (s * inv * pg[:, p]).astype(BF16)
            return carry

        lax.fori_loop(0, CHUNK // 16, some, 0)

    sent = []

    def send(src, dst, ssem, rsem, device):
        c = pltpu.make_async_remote_copy(
            src_ref=src, dst_ref=dst, send_sem=ssem, recv_sem=rsem,
            device_id=device, device_id_type=MESH,
        )
        c.start()
        sent.append(c)

    def arrived(dst, ssem, rsem):
        pltpu.make_async_remote_copy(
            src_ref=dst, dst_ref=dst, send_sem=ssem, recv_sem=rsem,
            device_id=other, device_id_type=MESH,
        ).wait_recv()

    def piece(k, which, rows):
        return tok.at[k, pl.ds(which * ROWS + rows[0], rows[1])]

    def pieces(k):
        return LAST if k == WINDOW - 1 else WHOLE

    def passing(t, rows):
        return transit.at[t, pl.ds(rows[0], rows[1])]

    def to_outer(src, k, i):
        j = (k - 1) * CHUNKS + i
        send(src, piece(k, 0, pieces(k)[i]), os_.at[j], or_.at[j], outer)

    def to_mate(src, t, i):
        j = t * CHUNKS + i
        send(src, passing(t, WHOLE[i]), ts.at[j], tr.at[j], mate)

    def to_other(k, i):
        j = k * CHUNKS + i
        rows = pieces(k)[i]
        send(piece(k, 0, rows), piece(k, 1, rows), ds_.at[j], dr.at[j], other)

    def own_out(c):
        to_outer(piece(0, 0, WHOLE[c]), 1, c)
        to_mate(piece(0, 0, WHOLE[c]), 0, c)
        to_other(0, c)

    def from_outer(k, i):
        j = (k - 1) * CHUNKS + i
        arrived(piece(k, 0, pieces(k)[i]), os_.at[j], or_.at[j])
        if k == 1:
            to_mate(piece(1, 0, WHOLE[i]), 1, i)
        to_other(k, i)

    def from_mate(t, c):
        j = t * CHUNKS + c
        arrived(passing(t, WHOLE[c]), ts.at[j], tr.at[j])
        for i, rows in enumerate(pieces(t + 2)):
            if WHOLE[c][0] <= rows[0] < WHOLE[c][0] + CHUNK:
                to_outer(passing(t, rows), t + 2, i)

    def from_other(k, i):
        j = k * CHUNKS + i
        arrived(piece(k, 1, pieces(k)[i]), ds_.at[j], dr.at[j])

    weights = (w0, w1)
    rings = {"A": ("x", 0, 0, 0), "B": ("y", 0, 1, 1)}
    for j in range(SIDE):
        rings[("A", j)] = ("y", j, 0, 2 + j)
        rings[("B", j)] = ("x", j, 1, 2 + SIDE + j)

    def w_rows(m, ring, step, start, count):
        axis, j, half, _ = rings[ring]
        dx, dy = (step, j) if axis == "x" else (j, step)
        owner = up_by(y, SIDE - dy, SIDE) * SIDE + up_by(x, SIDE - dx, SIDE)
        first = pl.multiple_of(owner * SHARD + half * HALF + start, QUARTER)
        return weights[m].at[pl.ds(first, count)]

    def w_send(m, ring, step, start, count, way, i):
        axis, _, _, r = rings[ring]
        ref = w_rows(m, ring, step, start, count)
        send(ref, ref, ws.at[m, r, i], wr.at[m, r, i], along[(axis, way)])

    def w_begin(m, *names):
        for ring in names:
            w_send(m, ring, 0, 0, HALF, 0, 0)
            w_send(m, ring, 0, 0, HALF, 1, 1)

    def w_arrived(m, ring, step, start, count, i):
        r = rings[ring][3]
        arrived(w_rows(m, ring, step, start, count), ws.at[m, r, i], wr.at[m, r, i])

    def w_near(m, *names):
        for ring in names:
            w_arrived(m, ring, 1, 0, HALF, 0)
            w_send(m, ring, 1, 0, QUARTER, 0, 2)
            w_arrived(m, ring, SIDE - 1, 0, HALF, 1)
            w_send(m, ring, SIDE - 1, QUARTER, QUARTER, 1, 3)

    def w_far(m, *names):
        for ring in names:
            w_arrived(m, ring, 2, 0, QUARTER, 2)
            w_arrived(m, ring, 2, QUARTER, QUARTER, 3)

    halves = ("A", "B")

    def w_give():
        for i, ring in enumerate(halves):
            send(w_rows(0, ring, 0, 0, HALF), w_rows(1, ring, 0, 0, HALF), xs.at[i], xr.at[i], mate)

    def w_taken(i):
        arrived(w_rows(1, halves[i], 0, 0, HALF), xs.at[i], xr.at[i])

    def first_row(which):
        return (core if which == 0 else 1 - core) * ROWS

    def project(m, k, spans):
        def tile(j, carry):
            cols = pl.ds(pl.multiple_of(j * 256, 256), 256)
            mine = pl.ds(pl.multiple_of(j * 128, 128), 128)
            parts = [tok[k, pl.ds(a, n), :] for a, n in spans]
            lhs = parts[0] if len(parts) == 1 else jnp.concatenate(parts, axis=0)
            both = jnp.dot(lhs, weights[m][:, cols], preferred_element_type=F32)
            gate = both[:, :128] * scales[m, j, 0:1]
            up = both[:, 128:] * scales[m, j, 1:2]
            out = (gate / (1.0 + jnp.exp(-gate)) * up).astype(BF16)
            at = 0
            for a, n in spans:
                while n > 0:
                    size = min(n, ROWS - a % ROWS)
                    to = first_row(a // ROWS) + a % ROWS
                    if m == 0:
                        to = pl.multiple_of(chip(-k) * 2 * ROWS + to, 16)
                        hidden[pl.ds(to, size), mine] = out[at:at + size]
                    else:
                        to = pl.multiple_of(to, 16)
                        given[k, pl.ds(to, size), mine] = out[at:at + size]
                    a, n, at = a + size, n - size, at + size
            return carry

        lax.fori_loop(0, TILES, tile, 0)

    def both_cores(rows):
        return tuple((which * ROWS + rows[0], rows[1]) for which in (0, 1))

    parcels = [(k, 0, 2 * ROWS) for k in range(WINDOW - 1)]
    splits = ((0, 64), (64, 48), (112, 16))
    for rows in splits:
        parcels += [(WINDOW - 1, which * ROWS + rows[0], rows[1]) for which in (0, 1)]

    def give(i):
        k, first, count = parcels[i]
        to = pl.multiple_of(chip(-k) * 2 * ROWS + first, 16)
        send(
            given.at[k, pl.ds(first, count)], hidden.at[pl.ds(to, count)],
            rs.at[i], rr.at[i], mate,
        )

    def take(i):
        k, first, count = parcels[i]
        to = pl.multiple_of(chip(1 + k) * 2 * ROWS + first, 16)
        arrived(hidden.at[pl.ds(to, count)], rs.at[i], rr.at[i])

    loads["gw"].wait()
    loads["uw"].wait()
    own = pl.ds(pl.multiple_of(fs * SHARD, SHARD), SHARD)
    for j in range(TILES):
        w0[own, j * 256:j * 256 + 128] = gate_v[:, j * 128:(j + 1) * 128].astype(BF16)
        w0[own, j * 256 + 128:(j + 1) * 256] = up_v[:, j * 128:(j + 1) * 128].astype(BF16)
    loads["mg"].wait()
    loads["pg"].wait()
    norm(0)
    pl.semaphore_wait(barrier, len(neighbours))
    w_give()
    w_begin(0, "A", "B", ("A", 0), ("B", 0))
    own_out(0)
    for c in range(1, CHUNKS):
        norm(c)
        if c > 1:
            own_out(c - 1)
    loads["gs"].wait()
    loads["us"].wait()
    send(gs, gs1, xs.at[2], xr.at[2], mate)
    send(us, us1, xs.at[3], xr.at[3], mate)
    own_out(CHUNKS - 1)

    w_near(0, "A", "B")
    w_taken(0)
    w_begin(1, "A")
    from_outer(1, 0)
    w_taken(1)
    w_begin(1, "B", ("A", 0), ("B", 0))
    from_outer(1, 1)
    from_mate(0, 0)
    w_near(1, "A", "B")
    w_begin(1, ("A", 1), ("A", 3), ("B", 1), ("B", 3))
    arrived(gs1, xs.at[2], xr.at[2])
    arrived(us1, xs.at[3], xr.at[3])
    for m, (g, u) in enumerate(((gs, us), (gs1, us1))):
        for j in range(TILES):
            scales[m, j, 0] = g[j * 128:(j + 1) * 128]
            scales[m, j, 1] = u[j * 128:(j + 1) * 128]
    from_outer(1, 2)
    w_near(1, ("A", 0), ("B", 0))
    w_far(1, "A", "B")
    w_begin(1, ("A", 2), ("B", 2))
    from_mate(0, 1)
    from_outer(1, 3)
    w_near(1, ("A", 1), ("B", 1))
    from_mate(0, 2)
    w_near(1, ("A", 3), ("B", 3))
    from_outer(2, 0)
    from_mate(0, 3)
    w_near(1, ("A", 2), ("B", 2))
    w_begin(0, ("A", 1), ("A", 3), ("B", 1), ("B", 3))
    w_near(0, ("A", 0), ("B", 0))
    w_far(0, "A", "B")
    w_begin(0, ("A", 2), ("B", 2))
    from_outer(2, 1)
    from_mate(1, 0)
    for j in (0, 1, 3, 2):
        w_far(1, ("A", j), ("B", j))

    def all_of(k):
        for i in range(len(pieces(k))):
            from_other(k, i)

    full = ((0, 2 * ROWS),)
    all_of(0)
    project(1, 0, full)
    from_outer(2, 2)
    from_mate(1, 1)
    w_near(0, ("A", 1), ("B", 1))
    all_of(1)
    project(1, 1, full)
    give(0)
    from_outer(2, 3)
    from_mate(1, 2)
    w_near(0, ("A", 3), ("B", 3))
    all_of(2)
    project(1, 2, full)
    give(1)
    from_outer(3, 0)
    from_mate(1, 3)
    w_near(0, ("A", 2), ("B", 2))
    give(2)
    from_outer(3, 1)
    from_other(3, 0)
    from_other(3, 1)
    project(1, 3, both_cores(splits[0]))
    for j in (0, 1, 3, 2):
        w_far(0, ("A", j), ("B", j))
    give(3)
    give(4)
    project(0, 0, full)
    project(0, 1, full)
    from_outer(3, 2)
    from_outer(3, 3)
    project(0, 2, full)
    from_outer(3, 4)
    from_other(3, 2)
    from_other(3, 3)
    project(1, 3, both_cores(splits[1]))
    from_other(3, 4)
    project(1, 3, both_cores(splits[2]))
    give(5)
    give(6)
    give(7)
    give(8)
    project(0, 3, full)
    for i in range(len(parcels)):
        take(i)

    for c in sent:
        c.wait_send()


def on_device(
    stream_in, mixer_out, mix_gain, pre_gain, gate_weight, up_weight, gate_scale, up_scale
):
    any_ = pl.BlockSpec(memory_space=pltpu.HBM)
    dma = pltpu.SemaphoreType.DMA
    return pl.pallas_call(
        kernel,
        name="gathered_projections",
        out_shape=(
            jax.ShapeDtypeStruct((DEEP * 2 * ROWS, COLS), BF16),
            jax.ShapeDtypeStruct((ROWS, D), BF16),
        ),
        in_specs=[any_] * 8,
        out_specs=(pl.BlockSpec(memory_space=pltpu.VMEM),) * 2,
        scratch_shapes=[
            pltpu.VMEM((WINDOW, 2 * ROWS, D), BF16),
            pltpu.VMEM((2, ROWS, D), BF16),
            pltpu.VMEM((D, 2 * COLS), BF16),
            pltpu.VMEM((D, 2 * COLS), BF16),
            pltpu.VMEM((ROWS, D), BF16),
            pltpu.VMEM((ROWS, D), BF16),
            pltpu.VMEM((SHARD, COLS), F32),
            pltpu.VMEM((SHARD, COLS), F32),
            pltpu.VMEM((1, D), F32),
            pltpu.VMEM((1, D), F32),
            pltpu.VMEM((COLS,), F32),
            pltpu.VMEM((COLS,), F32),
            pltpu.VMEM((COLS,), F32),
            pltpu.VMEM((COLS,), F32),
            pltpu.VMEM((2, TILES, 2, 128), F32),
            pltpu.VMEM((WINDOW, 2 * ROWS, COLS), BF16),
            dma((6 + 2 * CHUNKS,)),
            dma((3 * CHUNKS + 1,)),
            dma((3 * CHUNKS + 1,)),
            dma((2 * CHUNKS,)),
            dma((2 * CHUNKS,)),
            dma((WINDOW * CHUNKS + 1,)),
            dma((WINDOW * CHUNKS + 1,)),
            dma((4,)),
            dma((4,)),
            dma((WINDOW + 5,)),
            dma((WINDOW + 5,)),
            dma((2, 2 + 2 * SIDE, 4)),
            dma((2, 2 + 2 * SIDE, 4)),
        ],
        compiler_params=pltpu.CompilerParams(
            collective_id=0, has_side_effects=True, vmem_limit_bytes=40 * 2**20
        ),
    )(*(
        pltpu.with_memory_space_constraint(a, pltpu.HBM)
        for a in (
            stream_in, mixer_out, mix_gain.reshape(1, -1), pre_gain.reshape(1, -1),
            gate_weight, up_weight, gate_scale, up_scale,
        )
    ))


def solution(mesh):
    return jax.shard_map(
        on_device,
        mesh=mesh,
        in_specs=(
            P(("fs", "tp"), None),
            P(("fs", "tp"), None),
            P(),
            P(),
            P("fs", "tp"),
            P("fs", "tp"),
            P("tp"),
            P("tp"),
        ),
        out_specs=(P("fs", "tp"), P(("fs", "tp"), None)),
        check_vma=False,
    )
```

time: 98.9 us -> 91.9 us (0.929)
  Pallas kernels: 95.9 us -> 89 us
    pallas_call x1, Pallas kernels: 95.9 us -> 89 us  [on_device(): pl.pallas_call(kernel, name='gathered_projections', out_shape=(jax.ShapeD...]
where the time goes in v3:
time: 91.9 us; the launch traced here: 91.8 us
  Pallas kernels  89 us (97%)
  local copies, waits for them, and re-layouts  2.11 us (2%)
    pallas_call x1, Pallas kernels, on_device(): pl.pallas_call(kernel, name='gathered_projections', out_shape=(jax.ShapeD...  89 us
    unnamed x2, local copies, waits for them, and re-layouts  2.11 us

profile of v3, /device:TPU:1, one launch (start us, length us, event | category | flops | bytes accessed | tf_op | source)
XLA Modules:
  0.0 91.8 jit_solution(1678059650670138983)
XLA Ops:
  0.6 89.0 %gathered_projections.1 = (bf16[2048,384]{1,0:T(8,128)(2,1)S(1)}, bf16[128,4096]{1,0:T(8,128)(2,1)S(1)}) custom-call(bf16[128,4096]{1,0:T(8,128)(2,1)} %stream_in.1, bf16[128,4096]{1,0:T(8,128)(2,1)} %mixer_out.1, f32[1,4096]{1,0:T(1,128)} %bitcast.2, f32[1,4096]{1,0:T(1,128)} %bitcast.3, f32[256,384]{1,0:T(8,128)} %gate_w.1, f32[256,384]{1,0:T(8,128)} %up_w.1, ...), custom_call_target="tpu_custom_call" | custom-call | tf_op jit(solution)/shard_map/gathered_projections/pallas_call | solution.py:388
  89.7 1.1 %copy.12 = bf16[2048,384]{1,0:T(8,128)(2,1)} copy(bf16[2048,384]{1,0:T(8,128)(2,1)S(1)} %get-tuple-element.4) | data formatting | bytes 3145728
  90.8 1.0 %copy.13 = bf16[128,4096]{1,0:T(8,128)(2,1)} copy(bf16[128,4096]{1,0:T(8,128)(2,1)S(1)} %get-tuple-element.5) | data formatting | bytes 2097152

commit v4 on v3

--- a/solution.py
+++ b/solution.py
@@ -33,7 +33,7 @@
     stream_in, mixer_out, mix_gain, pre_gain, gate_w, up_w, gate_s, up_s,
     hidden, stream,
     tok, transit, w0, w1, stream_v, mixer_v, gate_v, up_v, mg, pg, gs, us, gs1, us1,
-    scales, given,
+    scales, given, partial,
     in_sem, os_, or_, ts, tr, ds_, dr, xs, xr, rs, rr, ws, wr,
 ):
     fs, tp = lax.axis_index("fs"), lax.axis_index("tp")
@@ -65,14 +65,15 @@
         c.start()
         loads[name] = c
 
-    load("gw", gate_w, gate_v)
-    load("uw", up_w, up_v)
     load("mg", mix_gain, mg)
-    load("pg", pre_gain, pg)
     for c in range(CHUNKS):
         rows = pl.ds(c * CHUNK, CHUNK)
         load(("m", c), mixer_out.at[rows], mixer_v.at[rows])
         load(("s", c), stream_in.at[rows], stream_v.at[rows])
+        if c == 0:
+            load("pg", pre_gain, pg)
+            load("gw", gate_w, gate_v)
+            load("uw", up_w, up_v)
     load("gs", gate_s, gs)
     load("us", up_s, us)
 
@@ -216,40 +217,64 @@
     def w_taken(i):
         arrived(w_rows(1, halves[i], 0, 0, HALF), xs.at[i], xr.at[i])
 
+    full = ((0, 2 * ROWS),)
+
     def first_row(which):
         return (core if which == 0 else 1 - core) * ROWS
 
+    def store(m, k, spans, j, both):
+        mine = pl.ds(j * 128, 128)
+        gate = both[:, :128] * scales[m, j, 0:1]
+        up = both[:, 128:] * scales[m, j, 1:2]
+        out = (gate / (1.0 + jnp.exp(-gate)) * up).astype(BF16)
+        at = 0
+        for a, n in spans:
+            while n > 0:
+                size = min(n, ROWS - a % ROWS)
+                to = first_row(a // ROWS) + a % ROWS
+                if m == 0:
+                    to = pl.multiple_of(chip(-k) * 2 * ROWS + to, 16)
+                    hidden[pl.ds(to, size), mine] = out[at:at + size]
+                else:
+                    to = pl.multiple_of(to, 16)
+                    given[k, pl.ds(to, size), mine] = out[at:at + size]
+                a, n, at = a + size, n - size, at + size
+
     def project(m, k, spans):
-        def tile(j, carry):
-            cols = pl.ds(pl.multiple_of(j * 256, 256), 256)
-            mine = pl.ds(pl.multiple_of(j * 128, 128), 128)
+        for j in range(TILES):
             parts = [tok[k, pl.ds(a, n), :] for a, n in spans]
             lhs = parts[0] if len(parts) == 1 else jnp.concatenate(parts, axis=0)
-            both = jnp.dot(lhs, weights[m][:, cols], preferred_element_type=F32)
-            gate = both[:, :128] * scales[m, j, 0:1]
-            up = both[:, 128:] * scales[m, j, 1:2]
-            out = (gate / (1.0 + jnp.exp(-gate)) * up).astype(BF16)
-            at = 0
-            for a, n in spans:
-                while n > 0:
-                    size = min(n, ROWS - a % ROWS)
-                    to = first_row(a // ROWS) + a % ROWS
-                    if m == 0:
-                        to = pl.multiple_of(chip(-k) * 2 * ROWS + to, 16)
-                        hidden[pl.ds(to, size), mine] = out[at:at + size]
-                    else:
-                        to = pl.multiple_of(to, 16)
-                        given[k, pl.ds(to, size), mine] = out[at:at + size]
-                    a, n, at = a + size, n - size, at + size
-            return carry
-
-        lax.fori_loop(0, TILES, tile, 0)
+            store(m, k, spans, j, jnp.dot(
+                lhs, weights[m][:, j * 256:(j + 1) * 256], preferred_element_type=F32
+            ))
+
+    def features(steps):
+        starts = []
+        for step in steps:
+            left, below = up_by(x, SIDE - step, SIDE), up_by(y, SIDE - step, SIDE)
+            starts += [(i * SIDE + left) * SHARD for i in range(SIDE)]
+            starts += [(below * SIDE + i) * SHARD + HALF for i in range(SIDE)]
+        return [pl.ds(pl.multiple_of(f, HALF), HALF) for f in starts]
+
+    def project_part(k, steps, last):
+        for j in range(TILES):
+            cols = slice(j * 256, (j + 1) * 256)
+            fs_ = features(steps)
+            both = jnp.dot(
+                jnp.concatenate([tok[k, :, f] for f in fs_], axis=1),
+                jnp.concatenate([w0[f, cols] for f in fs_], axis=0),
+                preferred_element_type=F32,
+            )
+            if last:
+                store(0, k, full, j, partial[k, :, cols] + both)
+            else:
+                partial[k, :, cols] = both
 
     def both_cores(rows):
         return tuple((which * ROWS + rows[0], rows[1]) for which in (0, 1))
 
     parcels = [(k, 0, 2 * ROWS) for k in range(WINDOW - 1)]
-    splits = ((0, 64), (64, 48), (112, 16))
+    splits = ((0, 96), (96, 32))
     for rows in splits:
         parcels += [(WINDOW - 1, which * ROWS + rows[0], rows[1]) for which in (0, 1)]
 
@@ -266,19 +291,21 @@
         to = pl.multiple_of(chip(1 + k) * 2 * ROWS + first, 16)
         arrived(hidden.at[pl.ds(to, count)], rs.at[i], rr.at[i])
 
+    loads["mg"].wait()
+    loads["pg"].wait()
+    norm(0)
     loads["gw"].wait()
     loads["uw"].wait()
     own = pl.ds(pl.multiple_of(fs * SHARD, SHARD), SHARD)
     for j in range(TILES):
         w0[own, j * 256:j * 256 + 128] = gate_v[:, j * 128:(j + 1) * 128].astype(BF16)
         w0[own, j * 256 + 128:(j + 1) * 256] = up_v[:, j * 128:(j + 1) * 128].astype(BF16)
-    loads["mg"].wait()
-    loads["pg"].wait()
-    norm(0)
     pl.semaphore_wait(barrier, len(neighbours))
+    to_outer(piece(0, 0, WHOLE[0]), 1, 0)
     w_give()
+    to_mate(piece(0, 0, WHOLE[0]), 0, 0)
+    to_other(0, 0)
     w_begin(0, "A", "B", ("A", 0), ("B", 0))
-    own_out(0)
     for c in range(1, CHUNKS):
         norm(c)
         if c > 1:
@@ -320,7 +347,6 @@
     w_begin(0, ("A", 1), ("A", 3), ("B", 1), ("B", 3))
     w_near(0, ("A", 0), ("B", 0))
     w_far(0, "A", "B")
-    w_begin(0, ("A", 2), ("B", 2))
     from_outer(2, 1)
     from_mate(1, 0)
     for j in (0, 1, 3, 2):
@@ -330,12 +356,12 @@
         for i in range(len(pieces(k))):
             from_other(k, i)
 
-    full = ((0, 2 * ROWS),)
     all_of(0)
     project(1, 0, full)
     from_outer(2, 2)
     from_mate(1, 1)
     w_near(0, ("A", 1), ("B", 1))
+    w_begin(0, ("A", 2), ("B", 2))
     all_of(1)
     project(1, 1, full)
     give(0)
@@ -346,38 +372,52 @@
     project(1, 2, full)
     give(1)
     from_outer(3, 0)
+    for j in (0, 1):
+        w_far(0, ("A", j), ("B", j))
+    project_part(0, (0, 1), False)
+    give(2)
     from_mate(1, 3)
+    project_part(1, (0, 1), False)
     w_near(0, ("A", 2), ("B", 2))
-    give(2)
     from_outer(3, 1)
-    from_other(3, 0)
-    from_other(3, 1)
+    project_part(2, (0, 1), False)
+    from_outer(3, 2)
+    for i in range(3):
+        from_other(3, i)
     project(1, 3, both_cores(splits[0]))
-    for j in (0, 1, 3, 2):
+    for j in (3, 2):
         w_far(0, ("A", j), ("B", j))
+    project_part(0, (3, 2), True)
+    from_outer(3, 3)
     give(3)
     give(4)
-    project(0, 0, full)
-    project(0, 1, full)
-    from_outer(3, 2)
-    from_outer(3, 3)
-    project(0, 2, full)
+    project_part(1, (3, 2), True)
+    project_part(2, (3, 2), True)
     from_outer(3, 4)
-    from_other(3, 2)
     from_other(3, 3)
+    from_other(3, 4)
     project(1, 3, both_cores(splits[1]))
-    from_other(3, 4)
-    project(1, 3, both_cores(splits[2]))
     give(5)
     give(6)
-    give(7)
-    give(8)
     project(0, 3, full)
     for i in range(len(parcels)):
         take(i)
 
     for c in sent:
         c.wait_send()
+
+
+def finish(hidden, stream, hidden_out, stream_out, sems):
+    copies = []
+    for src, dst in ((hidden, hidden_out), (stream, stream_out)):
+        rows = src.shape[0] // 4
+        for i in range(4):
+            part = pl.ds(i * rows, rows)
+            copies.append(pltpu.make_async_copy(src.at[part], dst.at[part], sems.at[len(copies)]))
+    for c in copies:
+        c.start()
+    for c in copies:
+        c.wait()
 
 
 def on_device(
@@ -385,7 +425,7 @@
 ):
     any_ = pl.BlockSpec(memory_space=pltpu.HBM)
     dma = pltpu.SemaphoreType.DMA
-    return pl.pallas_call(
+    hidden, stream = pl.pallas_call(
         kernel,
         name="gathered_projections",
         out_shape=(
@@ -411,6 +451,7 @@
             pltpu.VMEM((COLS,), F32),
             pltpu.VMEM((2, TILES, 2, 128), F32),
             pltpu.VMEM((WINDOW, 2 * ROWS, COLS), BF16),
+            pltpu.VMEM((WINDOW - 1, 2 * ROWS, 2 * COLS), F32),
             dma((6 + 2 * CHUNKS,)),
             dma((3 * CHUNKS + 1,)),
             dma((3 * CHUNKS + 1,)),
@@ -420,8 +461,8 @@
             dma((WINDOW * CHUNKS + 1,)),
             dma((4,)),
             dma((4,)),
-            dma((WINDOW + 5,)),
-            dma((WINDOW + 5,)),
+            dma((WINDOW + 3,)),
+            dma((WINDOW + 3,)),
             dma((2, 2 + 2 * SIDE, 4)),
             dma((2, 2 + 2 * SIDE, 4)),
         ],
@@ -435,6 +476,19 @@
             gate_weight, up_weight, gate_scale, up_scale,
         )
     ))
+    vmem = pl.BlockSpec(memory_space=pltpu.VMEM)
+    return pl.pallas_call(
+        finish,
+        name="results_out",
+        out_shape=(
+            jax.ShapeDtypeStruct(hidden.shape, BF16),
+            jax.ShapeDtypeStruct(stream.shape, BF16),
+        ),
+        in_specs=[vmem, vmem],
+        out_specs=(any_, any_),
+        scratch_shapes=[dma((8,))],
+        compiler_params=pltpu.CompilerParams(vmem_limit_bytes=16 * 2**20),
+    )(hidden, stream)
 
 
 def solution(mesh):

time: 91.9 us -> 89.9 us (0.978)
  local copies, waits for them, and re-layouts: 2.11 us -> 0 us
    unnamed x2 -> x0, local copies, waits for them, and re-layouts: 2.11 us -> none
    pallas_call x1, Pallas kernels: 89 us -> 87.4 us  [on_device(): pl.pallas_call(kernel, name='gathered_projections', out_shape=(jax.ShapeD...]
    pallas_call x0 -> x1, Pallas kernels: none -> 1.55 us  [on_device(): pl.pallas_call(finish, name='results_out', out_shape=(jax.ShapeDtypeStruc...]
where the time goes in v4:
time: 89.9 us; the launch traced here: 89.8 us
  Pallas kernels  89 us (99%)
    pallas_call x1, Pallas kernels, on_device(): pl.pallas_call(kernel, name='gathered_projections', out_shape=(jax.ShapeD...  87.4 us

profile of v4, /device:TPU:1, one launch (start us, length us, event | category | flops | bytes accessed | tf_op | source)
XLA Modules:
  0.0 89.8 jit_solution(6300874969961241116)
XLA Ops:
  0.6 87.4 %gathered_projections.1 = (bf16[2048,384]{1,0:T(8,128)(2,1)S(1)}, bf16[128,4096]{1,0:T(8,128)(2,1)S(1)}) custom-call(bf16[128,4096]{1,0:T(8,128)(2,1)} %stream_in.1, bf16[128,4096]{1,0:T(8,128)(2,1)} %mixer_out.1, f32[1,4096]{1,0:T(1,128)} %bitcast.2, f32[1,4096]{1,0:T(1,128)} %bitcast.3, f32[256,384]{1,0:T(8,128)} %gate_w.1, f32[256,384]{1,0:T(8,128)} %up_w.1, ...), custom_call_target="tpu_custom_call" | custom-call | tf_op jit(solution)/shard_map/gathered_projections/pallas_call | solution.py:428
  88.0 1.6 %results_out.1 = (bf16[2048,384]{1,0:T(8,128)(2,1)}, bf16[128,4096]{1,0:T(8,128)(2,1)}) custom-call(bf16[2048,384]{1,0:T(8,128)(2,1)S(1)} %get-tuple-element.4.hidden, bf16[128,4096]{1,0:T(8,128)(2,1)S(1)} %get-tuple-element.5.stream), custom_call_target="tpu_custom_call" | custom-call | tf_op jit(solution)/shard_map/results_out/pallas_call | solution.py:480

commit v5 on v4

--- a/solution.py
+++ b/solution.py
@@ -361,39 +361,38 @@
     from_outer(2, 2)
     from_mate(1, 1)
     w_near(0, ("A", 1), ("B", 1))
-    w_begin(0, ("A", 2), ("B", 2))
     all_of(1)
     project(1, 1, full)
     give(0)
     from_outer(2, 3)
     from_mate(1, 2)
     w_near(0, ("A", 3), ("B", 3))
+    w_begin(0, ("A", 2), ("B", 2))
     all_of(2)
     project(1, 2, full)
     give(1)
     from_outer(3, 0)
-    for j in (0, 1):
-        w_far(0, ("A", j), ("B", j))
-    project_part(0, (0, 1), False)
     give(2)
     from_mate(1, 3)
-    project_part(1, (0, 1), False)
+    for j in (0, 1, 3):
+        w_far(0, ("A", j), ("B", j))
+    project_part(0, (0, 1, 3), False)
+    from_outer(3, 1)
+    project_part(1, (0, 1, 3), False)
     w_near(0, ("A", 2), ("B", 2))
-    from_outer(3, 1)
-    project_part(2, (0, 1), False)
+    project_part(2, (0, 1, 3), False)
     from_outer(3, 2)
     for i in range(3):
         from_other(3, i)
     project(1, 3, both_cores(splits[0]))
-    for j in (3, 2):
-        w_far(0, ("A", j), ("B", j))
-    project_part(0, (3, 2), True)
+    w_far(0, ("A", 2), ("B", 2))
+    project_part(0, (2,), True)
     from_outer(3, 3)
     give(3)
     give(4)
-    project_part(1, (3, 2), True)
-    project_part(2, (3, 2), True)
+    project_part(1, (2,), True)
     from_outer(3, 4)
+    project_part(2, (2,), True)
     from_other(3, 3)
     from_other(3, 4)
     project(1, 3, both_cores(splits[1]))

time: 89.9 us -> 89.4 us (level)
  no operation moved by 1% of the time
where the time goes in v5:
time: 89.4 us; the launch traced here: 89.2 us
  Pallas kernels  88.4 us (99%)
    pallas_call x1, Pallas kernels, on_device(): pl.pallas_call(kernel, name='gathered_projections', out_shape=(jax.ShapeD...  86.8 us

profile of v5, /device:TPU:1, one launch (start us, length us, event | category | flops | bytes accessed | tf_op | source)
XLA Modules:
  0.0 89.2 jit_solution(8134008265447033019)
XLA Ops:
  0.6 86.8 %gathered_projections.1 = (bf16[2048,384]{1,0:T(8,128)(2,1)S(1)}, bf16[128,4096]{1,0:T(8,128)(2,1)S(1)}) custom-call(bf16[128,4096]{1,0:T(8,128)(2,1)} %stream_in.1, bf16[128,4096]{1,0:T(8,128)(2,1)} %mixer_out.1, f32[1,4096]{1,0:T(1,128)} %bitcast.2, f32[1,4096]{1,0:T(1,128)} %bitcast.3, f32[256,384]{1,0:T(8,128)} %gate_w.1, f32[256,384]{1,0:T(8,128)} %up_w.1, ...), custom_call_target="tpu_custom_call" | custom-call | tf_op jit(solution)/shard_map/gathered_projections/pallas_call | solution.py:427
  87.5 1.6 %results_out.1 = (bf16[2048,384]{1,0:T(8,128)(2,1)}, bf16[128,4096]{1,0:T(8,128)(2,1)}) custom-call(bf16[2048,384]{1,0:T(8,128)(2,1)S(1)} %get-tuple-element.4.hidden, bf16[128,4096]{1,0:T(8,128)(2,1)S(1)} %get-tuple-element.5.stream), custom_call_target="tpu_custom_call" | custom-call | tf_op jit(solution)/shard_map/results_out/pallas_call | solution.py:479
